TPU v7x, 32 devices: a whole 2x2x4 slice. The times are simulated.
32 devices in a mesh: grp: 2 (over y), dp: 2 (over x), kv: 4 (over z), tp: 2 (over core).
Axes of the slice: x: 2, y: 2, z: 4, core: 2. Of those that a mesh axis runs over, the one named last changes fastest.
Arguments:
- candidate_vectors: bfloat16 [128, 4, 2048], P(('grp', 'dp'), None, ('kv', 'tp')), parts along dimension 0, may hold values from -6 to 6
- leading_scaling_factor: bfloat16 [2048], replicated, may hold values from 0.099609375 to 1.8984375
- lane_feed_matrix: bfloat16 [2048, 32, 2, 64], P(None, 'kv', 'tp')
- final_valve_matrix: bfloat16 [2048, 32, 2, 64], P(None, 'kv', 'tp'), may hold values from -0.125 to 0.125
- increment_matrix: bfloat16 [2048, 32, 2], replicated, may hold values from -0.125 to 0.125
- entry_basis_matrix: bfloat16 [2048, 2, 128], P(None, 'tp'), may hold values from -0.125 to 0.125
- readout_basis_matrix: bfloat16 [2048, 2, 128], P(None, 'tp'), may hold values from -0.125 to 0.125
- lane_feed_kernel: float32 [4, 32, 2, 64], P(None, 'kv', 'tp'), may hold values from -3 to 3
- entry_basis_kernel: float32 [4, 2, 128], P(None, 'tp'), may hold values from -3 to 3
- readout_basis_kernel: float32 [4, 2, 128], P(None, 'tp'), may hold values from -3 to 3
- increment_offset: float32 [32, 2], P('kv', 'tp'), may hold values from -4 to 1
- shrink_speed_exponent: float32 [32, 2], P('kv', 'tp'), may hold values from 0 to 2.8
- lane_bypass_factor: float32 [32, 2], P('kv', 'tp'), may hold values from 0.5 to 1.5
- final_linear_matrix: bfloat16 [32, 2, 64, 2048], P(None, None, None, ('kv', 'tp')), may hold values from -0.09375 to 0.09375
- hidden_carried_memory: float32 [128, 32, 2, 64, 128], P(('grp', 'dp'), 'kv', 'tp'), parts along dimension 0, may hold values from -0.6 to 0.6
- lane_filter_memory: bfloat16 [128, 7, 32, 2, 64], P(('grp', 'dp'), None, 'kv', 'tp'), parts along dimension 0, may hold values from -6 to 6
- entry_basis_memory: bfloat16 [128, 7, 2, 128], P(('grp', 'dp'), None, 'tp'), parts along dimension 0, may hold values from -6 to 6
- readout_basis_memory: bfloat16 [128, 7, 2, 128], P(('grp', 'dp'), None, 'tp'), parts along dimension 0, may hold values from -6 to 6
- predecessor_index: int32 [128, 4], P(('grp', 'dp')), parts along dimension 0, may hold values from -1 to 2, as said below
- admitted_counts: int32 [128], P(('grp', 'dp')), parts along dimension 0, may hold values from 0 to 4
- surplus_fading: float32 [128, 4, 32, 2], P(('grp', 'dp'), None, 'kv', 'tp'), parts along dimension 0, may hold values from -0.7 to 0, as said below
Outputs:
- mixed: bfloat16 [128, 4, 2048], P(('grp', 'dp'), None, ('kv', 'tp')), parts along dimension 0
There are 2 independent parts, one for each index of `grp`. A program takes and returns all parts, laid end to end along the dimension named above; an argument that names none is the same for every part. Nothing has to cross between parts.
Inputs may be any that keep to these rules, and one draw needn't show every extreme that they name: predecessor_index[s, j] is -1 or a smaller proposal index than j. `surplus_fading`: zero except at a few proposals and heads.
All inputs are finite; a program needn't handle non-finite values.
Results may differ from a plain program's by a relative error of at most 0.012.
Values may be sent and summed in bfloat16 or wider, within the bound.
A program may use at most 64 MiB of HBM per device.

v0:
```python
import jax
import jax.numpy as jnp
from jax import lax
from jax.sharding import PartitionSpec as P

D = 2048
HG = 32
G = 2
HD = 64
N = 128
CONV = 4
WIN = 7


HIGH = lax.Precision.HIGHEST


def lineage_tables(predecessor_index):
    seqs, props = predecessor_index.shape
    column = jnp.arange(props, dtype=jnp.int32)
    current = jnp.broadcast_to(column[None, :], (seqs, props))
    depth = jnp.zeros((seqs, props), jnp.int32)
    onehots = []
    for step in range(props):
        onehots.append((current[:, :, None] == column[None, None, :]).astype(jnp.float32))
        if step > 0:
            depth = depth + (current >= 0).astype(jnp.int32)
        upward = jnp.take_along_axis(predecessor_index, jnp.maximum(current, 0), axis=1)
        current = jnp.where(current >= 0, upward, -1)
    return (onehots, depth)


def conv_tree(current, saved, taps, onehots, depth, admitted_counts):
    slots = jnp.arange(saved.shape[1], dtype=jnp.int32)
    cur_f = current.astype(jnp.float32)
    saved_f = saved.astype(jnp.float32)
    total = jnp.zeros(cur_f.shape, jnp.float32)
    for lag in range(CONV):
        value = jnp.einsum("sji,sic->sjc", onehots[lag], cur_f, precision=HIGH)
        target = admitted_counts[:, None] + (CONV - 1) - (lag - depth)
        chosen = ((depth < lag)[:, :, None] & (slots[None, None, :] == target[:, :, None])).astype(
            jnp.float32
        )
        value = value + jnp.einsum("sjw,swc->sjc", chosen, saved_f, precision=HIGH)
        total = total + taps[CONV - 1 - lag] * value
    return jax.nn.silu(total)


def shards(
    candidate_vectors,
    leading_scaling_factor,
    lane_feed_matrix,
    final_valve_matrix,
    increment_matrix,
    entry_basis_matrix,
    readout_basis_matrix,
    lane_feed_kernel,
    entry_basis_kernel,
    readout_basis_kernel,
    increment_offset,
    shrink_speed_exponent,
    lane_bypass_factor,
    final_linear_matrix,
    hidden_carried_memory,
    lane_filter_memory,
    entry_basis_memory,
    readout_basis_memory,
    predecessor_index,
    admitted_counts,
    surplus_fading,
):
    seqs, props, feat_dev = candidate_vectors.shape
    heads_dev = increment_offset.shape[0]
    rows = seqs * props
    kv_index = lax.axis_index("kv")
    tp_index = lax.axis_index("tp")
    dt_own = lax.dynamic_slice(
        increment_matrix, (0, kv_index * heads_dev, tp_index), (D, heads_dev, 1)
    ).reshape(D, heads_dev)
    wx_flat = lane_feed_matrix.reshape(D, heads_dev * HD)
    wz_flat = final_valve_matrix.reshape(D, heads_dev * HD)
    wb_flat = entry_basis_matrix.reshape(D, N)
    wc_flat = readout_basis_matrix.reshape(D, N)
    piece = lax.all_gather(candidate_vectors, ("kv", "tp"), axis=2, tiled=True)
    width = piece.shape[2]
    piece_f = piece.astype(jnp.float32)
    gain = leading_scaling_factor.astype(jnp.float32)
    scaled = (piece_f * gain).astype(jnp.bfloat16).reshape(rows, width)

    def partial_dot(source, weight):
        return jnp.dot(source, weight, preferred_element_type=jnp.float32)

    x_acc = partial_dot(scaled, wx_flat)
    z_acc = partial_dot(scaled, wz_flat)
    dt_acc = partial_dot(scaled, dt_own)
    b_acc = partial_dot(scaled, wb_flat)
    c_acc = partial_dot(scaled, wc_flat)
    squares = jnp.sum(piece_f * piece_f, axis=2).reshape(rows)
    r_in = lax.rsqrt(squares / D + 1e-06)
    x_rows = (x_acc * r_in[:, None]).astype(jnp.bfloat16).reshape(seqs, props, heads_dev * HD)
    z_rows = (z_acc * r_in[:, None]).astype(jnp.bfloat16).reshape(seqs, props, heads_dev, 1, HD)
    dt_raw = (dt_acc * r_in[:, None]).reshape(seqs, props, heads_dev, 1)
    b_flat = (b_acc * r_in[:, None]).astype(jnp.bfloat16)
    c_flat = (c_acc * r_in[:, None]).astype(jnp.bfloat16)
    onehots, depth = lineage_tables(predecessor_index)
    x_conv = conv_tree(
        x_rows,
        lane_filter_memory.reshape(seqs, WIN, -1),
        lane_feed_kernel.reshape(CONV, -1),
        onehots,
        depth,
        admitted_counts,
    ).reshape(seqs, props, heads_dev, 1, HD)
    b_conv = conv_tree(
        b_flat.reshape(seqs, props, N),
        entry_basis_memory.reshape(seqs, WIN, N),
        entry_basis_kernel.reshape(CONV, N),
        onehots,
        depth,
        admitted_counts,
    ).reshape(seqs, props, 1, N)
    c_conv = conv_tree(
        c_flat.reshape(seqs, props, N),
        readout_basis_memory.reshape(seqs, WIN, N),
        readout_basis_kernel.reshape(CONV, N),
        onehots,
        depth,
        admitted_counts,
    ).reshape(seqs, props, 1, N)
    lineage = sum(onehots)
    lane_increment = jax.nn.softplus(dt_raw + increment_offset)
    fading_exponent = -jnp.exp(shrink_speed_exponent) * lane_increment + surplus_fading
    level = jnp.einsum("sji,sihg->sjhg", lineage, fading_exponent, precision=HIGH)
    gap = level[:, :, None] - level[:, None, :]
    weight = jnp.where(lineage[:, :, :, None, None] > 0, jnp.exp(jnp.minimum(gap, 0.0)), 0.0)
    scores = jnp.einsum("sjgn,sign->sjig", c_conv, b_conv, precision=HIGH)
    mixing = weight * scores[:, :, :, None, :] * lane_increment[:, None]
    y_rows = jnp.einsum("sjihg,sihgp->sjhgp", mixing, x_conv, precision=HIGH)
    y_rows = y_rows + jnp.exp(level)[..., None] * jnp.einsum(
        "shgpn,sjgn->sjhgp", hidden_carried_memory, c_conv, precision=HIGH
    )
    y_rows = y_rows + lane_bypass_factor[..., None] * x_conv
    gated = (
        (y_rows * jax.nn.silu(z_rows.astype(jnp.float32)))
        .astype(jnp.bfloat16)
        .reshape(rows, heads_dev * HD)
    )
    kv_count = lax.axis_size("kv")
    out_cols = final_linear_matrix.shape[3]
    out_flat = jnp.transpose(
        final_linear_matrix.reshape(kv_count, heads_dev, G, HD, out_cols), (0, 2, 1, 3, 4)
    ).reshape(HG * G * HD, out_cols)
    empty = jnp.zeros((rows, out_cols), jnp.float32)
    gated_f = gated.astype(jnp.float32)
    sumsq_start = lax.psum(jnp.sum(gated_f * gated_f, axis=1), ("kv", "tp"))
    product = jnp.dot(
        lax.all_gather(gated, ("kv", "tp"), axis=1, tiled=True),
        out_flat,
        preferred_element_type=jnp.float32,
    )
    sumsq = (empty, sumsq_start)[1]
    r_out = lax.rsqrt(sumsq / (HG * G * HD) + 1e-05)
    return (product * r_out[:, None]).astype(jnp.bfloat16).reshape(seqs, props, out_cols)


def solution(mesh):
    placed = (
        P(("grp", "dp"), None, ("kv", "tp")),
        P(),
        P(None, "kv", "tp", None),
        P(None, "kv", "tp", None),
        P(),
        P(None, "tp", None),
        P(None, "tp", None),
        P(None, "kv", "tp", None),
        P(None, "tp", None),
        P(None, "tp", None),
        P("kv", "tp"),
        P("kv", "tp"),
        P("kv", "tp"),
        P(None, None, None, ("kv", "tp")),
        P(("grp", "dp"), "kv", "tp", None, None),
        P(("grp", "dp"), None, "kv", "tp", None),
        P(("grp", "dp"), None, "tp", None),
        P(("grp", "dp"), None, "tp", None),
        P(("grp", "dp"), None),
        P(("grp", "dp")),
        P(("grp", "dp"), None, "kv", "tp"),
    )
    return jax.shard_map(
        shards,
        mesh=mesh,
        in_specs=placed,
        out_specs=P(("grp", "dp"), None, ("kv", "tp")),
        check_vma=False,
    )
```

profile of v0, /device:TPU:19, one launch (start us, length us, event | category | flops | bytes accessed | tf_op | source)
XLA Modules:
  0.0 123.8 jit_solution(8136422851500246056)
XLA Ops:
  6.8 0.5 copy-done.1
  7.4 1.5 %gather_fusion = s32[128]{0:T(128)S(1)} fusion(s32[32,4]{0,1:T(4,128)S(1)} %copy-done.1, s32[128]{0:T(128)S(1)} %reshape.376), kind=kCustom, calls=%fused_computation.clone | custom fusion | bytes 2048 | tf_op jit(solution)/shard_map/jit(take_along_axis)/gather | solution.py:28
  9.4 1.5 %gather_fusion.1 = s32[128]{0:T(128)S(1)} fusion(s32[32,4]{0,1:T(4,128)S(1)} %copy-done.1, s32[128]{0:T(128)S(1)} %reshape.381), kind=kCustom, calls=%fused_computation.1.clone | custom fusion | bytes 2048 | tf_op jit(solution)/shard_map/jit(take_along_axis)/gather | solution.py:28
  11.3 1.5 %gather_fusion.2 = s32[128]{0:T(128)S(1)} fusion(s32[32,4]{0,1:T(4,128)S(1)} %copy-done.1, s32[128]{0:T(128)S(1)} %reshape.386), kind=kCustom, calls=%fused_computation.2.clone | custom fusion | bytes 2048 | tf_op jit(solution)/shard_map/jit(take_along_axis)/gather | solution.py:28
  13.3 12.7 %all_gather.6 = bf16[32,4,2048]{2,1,0:T(4,128)(2,1)S(1)} all-gather(bf16[32,4,256]{2,1,0:T(4,128)(2,1)S(1)} %copy-done.7), channel_id=1, replica_groups=mesh['grp'=2,'dp'=2,'kv'=4,'tp'=2] {'kv','tp'}, dimensions={2}, use_global_device_ids=true | all-gather | bytes 589824 | tf_op jit(solution)/shard_map/all_gather | solution.py:84
  26.0 0.5 fusion.30
  26.8 1.3 %fusion.27 = bf16[128,128]{1,0:T(8,128)(2,1)S(1)} fusion(bf16[128,2048]{1,0:T(8,128)(2,1)S(1)} %reshape.317, bf16[2048,1,128]{2,0,1:T(8,128)(2,1)} %param.28, f32[128]{0:T(128)S(1)} %rsqrt.14), kind=kOutput, calls=%fused_computation.50 | convolution fusion | flops 67141632 | bytes 1081856 | tf_op jit(solution)/shard_map/dot_general | solution.py:91
  28.2 0.9 fusion.67
  29.0 0.9 fusion.70
  29.9 0.8 fusion.90
  30.7 0.9 fusion.73
  31.5 0.8 fusion.76
  32.3 1.3 %fusion.28 = bf16[128,128]{1,0:T(8,128)(2,1)S(1)} fusion(bf16[128,2048]{1,0:T(8,128)(2,1)S(1)} %reshape.317, bf16[2048,1,128]{2,0,1:T(8,128)(2,1)} %param.29, f32[128]{0:T(128)S(1)} %rsqrt.14), kind=kOutput, calls=%fused_computation.51 | convolution fusion | flops 67141632 | bytes 1081856 | tf_op jit(solution)/shard_map/dot_general | solution.py:91
  33.6 0.9 fusion.66
  34.5 0.9 fusion.69
  35.3 0.8 fusion.72
  36.2 0.8 fusion.75
  37.0 0.8 fusion.9
  37.9 1.0 fusion.68
  39.1 1.0 fusion.74
  40.8 0.7 copy.134
  42.1 1.3 %reshape.391 = bf16[32,7,512]{2,1,0:T(8,128)(2,1)S(1)} reshape(bf16[32,7,8,1,64]{4,2,3,1,0:T(8,128)(2,1)} %param.38) | data formatting | bytes 458752 | tf_op jit(solution)/shard_map/reshape | solution.py:108
  43.7 1.2 fusion.7
  45.9 1.0 reshape.321
  47.0 1.2 negate_bitcast_fusion
  48.2 0.6 slice_bitcast_fusion.4
  48.8 0.6 slice_bitcast_fusion
  49.5 0.9 constant_dynamic-slice_fusion
  50.9 0.9 copy.151
  51.8 1.1 fusion.26
  53.0 1.1 fusion.25
  54.1 1.1 fusion.23
  55.2 1.2 fusion.21
  56.4 1.1 fusion.19
  58.3 0.4 convolution_bitcast_fusion
  58.7 0.9 copy.149
  59.6 1.7 %fusion.124 = (f32[32,4,8]{2,1,0:T(4,128)}, f32[32,4,8]{2,1,0:T(4,128)S(1)}) fusion(f32[32,4,8,1]{2,1,0,3:T(4,128)S(1)} %copy.138, f32[32,4,8,1]{2,1,0,3:T(4,128)S(1)} %bitcast.125, f32[8]{0:T(128)S(1)} %bitcast.135, f32[8]{0:T(128)} %negate_bitcast_fusion, s32[32,4]{1,0:T(8,128)S(1)} %copy.132, s32[32,4]{1,0:T(8,128)S(1)} %copy.128, s32[32,4]{1,0:T(8,128)S(1)} %copy.124), kind=kOutput, calls=%fused_computation.189 | convolution fusion | flops 64000 | bytes 17984 | tf_op jit(solution)/shard_map/sji,sihg->sjhg/dot_general | solution.py:133
  61.6 2.4 %fusion.11 = f32[128,512]{1,0:T(8,128)S(1)} fusion(bf16[128,2048]{1,0:T(8,128)(2,1)S(1)} %reshape.317, bf16[2048,512]{0,1:T(8,128)(2,1)} %bitcast.122, f32[128]{0:T(128)S(1)} %rsqrt.14), kind=kOutput, calls=%fused_computation.22 | convolution fusion | flops 268632064 | bytes 2884096 | tf_op jit(solution)/shard_map/dot_general | solution.py:91
  64.1 0.9 reshape.341
  65.0 22.1 %fusion = f32[32,4,8,64]{3,1,2,0:T(4,128)S(1)} fusion(f32[32,8,1,64,128]{4,3,2,1,0:T(8,128)} %param.37, f32[32,4,128]{2,1,0:T(4,128)} %copy-done.6), kind=kOutput, calls=%fused_computation.3 | convolution fusion | flops 100663296 | bytes 8716288 | tf_op jit(solution)/shard_map/shgpn,sjgn->sjhgp/dot_general | solution.py:139
  87.2 2.1 %fusion.36 = f32[32,8,64,4]{2,3,1,0:T(4,128)S(1)} fusion(f32[32,4,8,64]{3,2,1,0:T(8,128)S(1)} %copy-done.3, f32[32,4,8]{1,2,0:T(8,128)S(1)} %copy-done.5, f32[32,4,4]{2,1,0:T(4,128)S(1)} %copy-done.10, f32[32,4,8]{1,2,0:T(8,128)S(1)} %copy.139, pred[32,4,4]{2,1,0:T(4,128)(4,1)S(1)} %copy-done.15), kind=kOutput, calls=%fused_computation.62 | convolution fusion | flops 3166208 | bytes 535040 | tf_op jit(solution)/shard_map/sjihg,sihgp->sjhgp/dot_general | solution.py:138
  89.3 0.6 multiply_reduce_fusion
  89.9 0.9 reshape.335
  90.9 3.2 %copy.155 = bf16[4,2,8,64,256]{4,3,2,1,0:T(8,128)(2,1)} copy(bf16[4,2,8,64,256]{4,3,1,2,0:T(8,128)(2,1)} %bitcast.123) | data formatting | bytes 4194304 | tf_op jit(solution)/shard_map/transpose | solution.py:150
  94.1 11.6 %psum.7 = f32[128]{0:T(128)S(1)} all-reduce(f32[128]{0:T(128)S(1)} %reduce_sum.22), channel_id=1, replica_groups=mesh['grp'=2,'dp'=2,'kv'=4,'tp'=2] {'kv','tp'}, use_global_device_ids=true, to_apply=%region_2.4 | all-reduce | flops 128 | bytes 1024 | tf_op jit(solution)/shard_map/psum | solution.py:155
  105.6 8.3 %all-gather.2.cloned.1.call-done = bf16[128,4096]{1,0:T(8,128)(2,1)} async-done(((bf16[128,512]{1,0:T(8,128)(2,1)}), bf16[128,4096]{1,0:T(8,128)(2,1)}) %all-gather.2.cloned.1.call-update) | async-done | bytes 1048592 | tf_op jit(solution)/shard_map/all_gather | solution.py:157
  114.0 2.4 %fusion.12 = bf16[128,256]{1,0:T(8,128)(2,1)S(1)} fusion(bf16[128,4096]{1,0:T(8,128)(2,1)} %all-gather.2.cloned.1.call-done, bf16[4096,256]{1,0:T(8,128)(2,1)} %bitcast.121, f32[128]{0:T(128)S(1)} %add_rsqrt_fusion.1), kind=kOutput, calls=%fused_computation.24 | convolution fusion | flops 268500992 | bytes 3211776 | tf_op jit(solution)/shard_map/dot_general | solution.py:156
  116.3 0.7 reshape.338
  (117 shorter events, 6.3 us)
Async XLA Ops:
  6.5 30.4 %copy-start = (bf16[2048,8,1,64]{0,3,2,1:T(8,128)(2,1)S(1)}, bf16[2048,8,1,64]{0,3,2,1:T(8,128)(2,1)}, u32[]{:S(2)}) copy-start(bf16[2048,8,1,64]{0,3,2,1:T(8,128)(2,1)} %param.25) | copy-start | bytes 6291460
  6.5 0.8 copy-start.1
  6.5 107.4 %all-gather.2.cloned.1.call-start = ((), (), s32[]{:S(2)}) async-start(), calls=%async_computation | async-start | bytes 1179648 | tf_op jit(solution)/shard_map/all_gather | solution.py:157
  11.3 1.9 %copy-start.16 = (bf16[2048]{0:T(1024)(128)(2,1)S(1)}, bf16[2048]{0:T(1024)(128)(2,1)}, u32[]{:S(2)}) copy-start(bf16[2048]{0:T(1024)(128)(2,1)} %param.24) | copy-start | bytes 12292
  11.3 2.0 %copy-start.7 = (bf16[32,4,256]{2,1,0:T(4,128)(2,1)S(1)}, bf16[32,4,256]{2,1,0:T(4,128)(2,1)}, u32[]{:S(2)}) copy-start(bf16[32,4,256]{2,1,0:T(4,128)(2,1)} %param.23) | copy-start | bytes 196612
  37.0 3.3 %copy-start.25 = (s32[32]{0:T(128)S(1)}, s32[32]{0:T(128)}, u32[]{:S(2)}) copy-start(s32[32]{0:T(128)} %param.42) | copy-start | bytes 388
  37.0 4.7 %copy-start.14 = (f32[4,8,1,64]{3,2,1,0:T(1,128)S(1)}, f32[4,8,1,64]{3,2,1,0:T(1,128)}, u32[]{:S(2)}) copy-start(f32[4,8,1,64]{3,2,1,0:T(1,128)} %param.30) | copy-start | bytes 24580
  43.4 1.8 %copy-start.4 = (f32[32,4,512]{2,1,0:T(4,128)S(1)}, f32[32,4,512]{2,1,0:T(4,128)}, u32[]{:S(2)}) copy-start(f32[32,4,512]{2,1,0:T(4,128)} %fusion.68) | copy-start | bytes 786436
  43.4 1.8 %copy-start.12 = (s32[32,4]{1,0:T(8,128)S(1)}, s32[32,4]{1,0:T(8,128)}, u32[]{:S(2)}) copy-start(s32[32,4]{1,0:T(8,128)} %copy.134) | copy-start | bytes 1540
  45.3 2.9 %copy-start.17 = (f32[4,1,128]{2,1,0:T(1,128)S(1)}, f32[4,1,128]{2,1,0:T(1,128)}, u32[]{:S(2)}) copy-start(f32[4,1,128]{2,1,0:T(1,128)} %param.31) | copy-start | bytes 6148
  45.3 3.5 %copy-start.18 = (f32[4,1,128]{2,1,0:T(1,128)S(1)}, f32[4,1,128]{2,1,0:T(1,128)}, u32[]{:S(2)}) copy-start(f32[4,1,128]{2,1,0:T(1,128)} %param.32) | copy-start | bytes 6148
  45.3 4.1 %copy-start.11 = (f32[32,4,8,1]{0,3,2,1:T(1,128)S(1)}, f32[32,4,8,1]{0,3,2,1:T(1,128)}, u32[]{:S(2)}) copy-start(f32[32,4,8,1]{0,3,2,1:T(1,128)} %param.43) | copy-start | bytes 12292
  45.7 5.1 %copy-start.19 = (f32[8,1]{0,1:T(1,128)S(1)}, f32[8,1]{0,1:T(1,128)}, u32[]{:S(2)}) copy-start(f32[8,1]{0,1:T(1,128)} %param.33) | copy-start | bytes 100
  47.0 9.4 %copy-start.9 = (f32[32,4,128]{2,1,0:T(4,128)S(1)}, f32[32,4,128]{2,1,0:T(4,128)}, u32[]{:S(2)}) copy-start(f32[32,4,128]{2,1,0:T(4,128)} %fusion.75) | copy-start | bytes 196612
  50.4 7.6 %copy-start.13 = (s32[32,4]{1,0:T(8,128)S(1)}, s32[32,4]{1,0:T(8,128)}, u32[]{:S(2)}) copy-start(s32[32,4]{1,0:T(8,128)} %copy.134) | copy-start | bytes 1540
  50.4 7.6 %copy-start.20 = (f32[128]{0:T(128)S(1)}, f32[128]{0:T(128)}, u32[]{:S(2)}) copy-start(f32[128]{0:T(128)} %get-tuple-element.28) | copy-start | bytes 1540
  50.8 7.0 %copy-start.21 = (f32[128]{0:T(128)S(1)}, f32[128]{0:T(128)}, u32[]{:S(2)}) copy-start(f32[128]{0:T(128)} %get-tuple-element.31) | copy-start | bytes 1540
  51.8 5.6 %copy-start.22 = (f32[128]{0:T(128)S(1)}, f32[128]{0:T(128)}, u32[]{:S(2)}) copy-start(f32[128]{0:T(128)} %get-tuple-element.29) | copy-start | bytes 1540
  51.8 5.7 %copy-start.24 = (bf16[32,7,1,128]{3,0,2,1:T(8,128)(2,1)S(1)}, bf16[32,7,1,128]{3,0,2,1:T(8,128)(2,1)}, u32[]{:S(2)}) copy-start(bf16[32,7,1,128]{3,0,2,1:T(8,128)(2,1)} %param.40) | copy-start | bytes 172036
  51.8 5.7 %copy-start.28 = (f32[32,4,128]{2,1,0:T(4,128)S(1)}, f32[32,4,128]{2,1,0:T(4,128)}, u32[]{:S(2)}) copy-start(f32[32,4,128]{2,1,0:T(4,128)} %fusion.72) | copy-start | bytes 196612
  51.8 5.9 %copy-start.27 = (f32[32,4,128]{2,1,0:T(4,128)S(1)}, f32[32,4,128]{2,1,0:T(4,128)}, u32[]{:S(2)}) copy-start(f32[32,4,128]{2,1,0:T(4,128)} %fusion.69) | copy-start | bytes 196612
  51.8 6.2 %copy-start.26 = (f32[32,4,128]{2,1,0:T(4,128)S(1)}, f32[32,4,128]{2,1,0:T(4,128)}, u32[]{:S(2)}) copy-start(f32[32,4,128]{2,1,0:T(4,128)} %fusion.66) | copy-start | bytes 196612
  58.3 3.3 %copy-start.6 = (f32[32,4,128]{2,1,0:T(4,128)}, f32[32,4,128]{2,1,0:T(4,128)S(1)}, u32[]{:S(2)}) copy-start(f32[32,4,128]{2,1,0:T(4,128)S(1)} %divide_multiply_fusion.1) | copy-start | bytes 196612
  65.0 22.1 %copy-start.3 = (f32[32,4,8,64]{3,2,1,0:T(8,128)S(1)}, f32[32,4,8,64]{3,2,1,0:T(8,128)}, u32[]{:S(2)}) copy-start(f32[32,4,8,64]{3,2,1,0:T(8,128)} %reshape.321) | copy-start | bytes 786436
  65.0 22.1 %copy-start.5 = (f32[32,4,8]{1,2,0:T(8,128)S(1)}, f32[32,4,8]{1,2,0:T(8,128)}, u32[]{:S(2)}) copy-start(f32[32,4,8]{1,2,0:T(8,128)} %copy.151) | copy-start | bytes 12292
  65.0 22.1 %copy-start.10 = (f32[32,4,4]{2,1,0:T(4,128)S(1)}, f32[32,4,4]{2,1,0:T(4,128)}, u32[]{:S(2)}) copy-start(f32[32,4,4]{2,1,0:T(4,128)} %copy.149) | copy-start | bytes 6148
  65.0 22.1 %copy-start.15 = (pred[32,4,4]{2,1,0:T(4,128)(4,1)S(1)}, pred[32,4,4]{2,1,0:T(4,128)(4,1)}, u32[]{:S(2)}) copy-start(pred[32,4,4]{2,1,0:T(4,128)(4,1)} %fusion.90) | copy-start | bytes 1540
  87.1 2.2 %copy-start.2 = (f32[32,4,8,1,64]{4,2,3,1,0:T(8,128)S(1)}, f32[32,4,8,1,64]{4,2,3,1,0:T(8,128)}, u32[]{:S(2)}) copy-start(f32[32,4,8,1,64]{4,2,3,1,0:T(8,128)} %reshape.341) | copy-start | bytes 786436
  87.2 2.2 %copy-start.8 = (f32[32,4,8]{2,1,0:T(4,128)S(1)}, f32[32,4,8]{2,1,0:T(4,128)}, u32[]{:S(2)}) copy-start(f32[32,4,8]{2,1,0:T(4,128)} %get-tuple-element.35) | copy-start | bytes 12292
  87.2 2.2 %copy-start.23 = (f32[8,1]{0,1:T(1,128)S(1)}, f32[8,1]{0,1:T(1,128)}, u32[]{:S(2)}) copy-start(f32[8,1]{0,1:T(1,128)} %param.35) | copy-start | bytes 100
Sparse Core Ops, SparseCore 0:
  90.9 23.0 all-gather.1
where the time goes:
time: 126 us; the launch traced here: 124 us
  matrix products  52.5 us (42%)
  blocking collectives  24.3 us (19%)
  local copies, waits for them, and re-layouts  21.2 us (17%)
  between operations  14 us (11%)
  waiting for transfers between devices  8.33 us (7%)
  other arithmetic  3.44 us (3%)
    dot_general x1, matrix products, shards(): jnp.einsum('shgpn,sjgn->sjhgp', hidden_carried_memory, c_conv, precision=...  22.1 us
    all_gather x1, blocking collectives, shards(): piece = lax.all_gather(candidate_vectors, ('kv', 'tp'), axis=2, tiled=True)  12.7 us
    psum x1, blocking collectives, shards(): sumsq_start = lax.psum(jnp.sum(gated_f * gated_f, axis=1), ('kv', 'tp'))  11.6 us
    dot_general x12, matrix products, conv_tree(): value = jnp.einsum('sji,sic->sjc', onehots[lag], cur_f, precision=HIGH)  9.14 us
    dot_general x12, matrix products, conv_tree(): value = value + jnp.einsum('sjw,swc->sjc', chosen, saved_f, precision=HIGH)  8.55 us
    all_gather x1, waiting for transfers between devices, shards(): lax.all_gather(gated, ('kv', 'tp'), axis=1, tiled=True)  8.31 us
    dot_general x5, matrix products, partial_dot(): return jnp.dot(source, weight, preferred_element_type=jnp.float32)  6.16 us
    gather x15, local copies, waits for them, and re-layouts, lineage_tables(): jnp.take_along_axis(predecessor_index, jnp.maximum(current, 0), axis=1)  5.63 us
  transfers between devices with their start and end apart: 1, of which 1 were waited for; matrix products, arithmetic and copies ran while one was open for 3% of the time, Pallas kernels for 0%

commit v1 on v0

v1 whole, which is shorter than its diff:
```python
import functools

import jax
import jax.numpy as jnp
from jax import lax
from jax.experimental import pallas as pl
from jax.experimental.pallas import tpu as pltpu
from jax.sharding import PartitionSpec as P

CONV = 4
MESH = pl.DeviceIdType.MESH
HIGH = lax.Precision.HIGHEST
F32 = jnp.float32
BF16 = jnp.bfloat16
NT = (((1,), (1,)), ((), ()))


def silu(value):
    return value * jax.nn.sigmoid(value)


def mixer_kernel(
    n, seqs, props, heads, hd, chunks, d_model, heads_all,
    x_hbm, gain_ref, wx_hbm, wz_hbm, dtw_ref, wb_hbm, wc_hbm,
    xtap_ref, btap_ref, ctap_ref, offset_ref, shrink_ref, bypass_ref,
    fl_hbm, st_hbm, xsave_ref, bsave_ref, csave_ref, pred_ref, adm_ref, fade_ref,
    out_ref,
    xg, gg, wx, wz, wb, wc, fl, st, acc_x, acc_z, xrow, cs, ys,
    load_sem, st_sem, own_sem, s1, r1, s1b, r1b, s2, r2, s2b, r2b,
):
    kv = lax.axis_index("kv")
    tp = lax.axis_index("tp")
    other = 1 - tp
    rows = seqs * props
    feat = x_hbm.shape[1]
    wide = heads * hd
    cw = wide // chunks
    hpc = heads // chunks

    own = pltpu.make_async_copy(x_hbm, xg.at[0, tp], own_sem)
    own.start()
    barrier = pltpu.get_barrier_semaphore()
    for step in range(1, n):
        pl.semaphore_signal(
            barrier, inc=1, device_id={"kv": lax.rem(kv + step, n)}, device_id_type=MESH
        )
    pl.semaphore_signal(barrier, inc=1, device_id={"tp": other}, device_id_type=MESH)

    loads = []
    for index, (src, dst) in enumerate(
        ((wb_hbm, wb), (wc_hbm, wc), (wx_hbm, wx), (wz_hbm, wz), (fl_hbm, fl))
    ):
        loads.append(pltpu.make_async_copy(src, dst, load_sem.at[index]))
    parts = st_sem.shape[0]
    span = seqs // parts
    st_loads = [
        pltpu.make_async_copy(
            st_hbm.at[pl.ds(part * span, span)], st.at[pl.ds(part * span, span)], st_sem.at[part]
        )
        for part in range(parts)
    ]
    for copy in loads[:4] + st_loads + loads[4:]:
        copy.start()

    pl.semaphore_wait(barrier, n)
    own.wait()

    def to_chip(src, dst, step, send, recv):
        return pltpu.make_async_remote_copy(
            src_ref=src, dst_ref=dst, send_sem=send, recv_sem=recv,
            device_id={"kv": lax.rem(kv + step, n)}, device_id_type=MESH,
        )

    def to_sibling(ref, send, recv):
        return pltpu.make_async_remote_copy(
            src_ref=ref, dst_ref=ref, send_sem=send, recv_sem=recv,
            device_id={"tp": other}, device_id_type=MESH,
        )

    order = sorted(range(1, n), key=lambda step: (min(step, n - step), step))
    first = {}
    for step in order:
        first[step] = to_chip(
            xg.at[0, tp], xg.at[n - step, tp], step, s1.at[step], r1.at[n - step]
        )
        first[step].start()
    first_sib = {0: to_sibling(xg.at[0, tp], s1b.at[0], r1b.at[0])}
    first_sib[0].start()

    eye = (
        lax.broadcasted_iota(jnp.int32, (seqs, seqs), 0)
        == lax.broadcasted_iota(jnp.int32, (seqs, seqs), 1)
    ).astype(F32)

    def turn(value):
        return lax.dot_general(eye, value, NT, precision=HIGH, preferred_element_type=F32)

    parent = turn(pred_ref[...].astype(F32))
    admitted = turn(adm_ref[...].astype(F32))[:, :1]
    current = [jnp.full((seqs, 1), float(j), F32) for j in range(props)]
    above = [parent[:, j : j + 1] for j in range(props)]
    onehot = {}
    depth = [jnp.zeros((seqs, 1), F32) for _ in range(props)]
    lineage = {}
    for lag in range(props):
        for j in range(props):
            for i in range(j + 1):
                onehot[lag, j, i] = (current[j] == float(i)).astype(F32)
                lineage[j, i] = lineage.get((j, i), 0.0) + onehot[lag, j, i]
            if lag > 0:
                depth[j] = depth[j] + (current[j] >= 0.0).astype(F32)
        for j in range(props):
            upward = jnp.full((seqs, 1), -1.0, F32)
            for i in range(j + 1):
                hit = onehot[lag, j, i]
                upward = upward + hit * (above[i] + 1.0)
            current[j] = upward
    depth_is = {
        (j, d): (depth[j] == float(d)).astype(F32) for j in range(props) for d in range(j + 1)
    }
    slots = xsave_ref.shape[0]
    pick = [(admitted == float(a)).astype(F32) for a in range(slots - CONV + 2)]

    def previous(save):
        return [
            sum(pick[a] * save(a + back) for a in range(len(pick)))
            for back in range(CONV - 1)
        ]

    def conv(slabs, prev, tap):
        result = []
        for j in range(props):
            total = tap(CONV - 1) * slabs[j]
            for lag in range(1, CONV):
                value = None
                for i in range(j - lag + 1):
                    term = onehot[lag, j, i] * slabs[i]
                    value = term if value is None else value + term
                for d in range(min(lag, j + 1)):
                    term = depth_is[j, d] * prev[CONV - 1 - lag + d]
                    value = term if value is None else value + term
                total = total + tap(CONV - 1 - lag) * value
            result.append(silu(total))
        return result

    for copy in loads[:4]:
        copy.wait()
    squares = jnp.zeros((rows, 1), F32)
    acc_b = jnp.zeros((rows, wb.shape[1]), F32)
    acc_c = jnp.zeros((rows, wc.shape[1]), F32)
    acc_dt = jnp.zeros((rows, heads), F32)
    for place, slot in enumerate([0] + [n - step for step in order]):
        if slot:
            to_chip(xg.at[0, tp], xg.at[slot, tp], 1, s1.at[0], r1.at[slot]).wait_recv()
            first_sib[slot] = to_sibling(xg.at[slot, tp], s1b.at[slot], r1b.at[slot])
            first_sib[slot].start()
        to_sibling(xg.at[slot, other], s1b.at[slot], r1b.at[slot]).wait_recv()
        chip = lax.rem(kv + slot, n)
        base = pl.multiple_of(chip * (2 * feat), 2 * feat)
        tokens = jnp.concatenate([xg[slot, 0], xg[slot, 1]], axis=1).astype(F32)
        squares = squares + jnp.sum(tokens * tokens, axis=1, keepdims=True)
        span_k = pl.ds(base, 2 * feat)
        scaled = (tokens * gain_ref[:, span_k].astype(F32)).astype(BF16)
        px = lax.dot_general(scaled, wx[:, span_k], NT, preferred_element_type=F32)
        pz = lax.dot_general(scaled, wz[:, span_k], NT, preferred_element_type=F32)
        if place == 0:
            acc_x[...] = px
            acc_z[...] = pz
        else:
            acc_x[...] += px
            acc_z[...] += pz
        acc_b = acc_b + jnp.dot(scaled, wb[span_k, :], preferred_element_type=F32)
        acc_c = acc_c + jnp.dot(scaled, wc[span_k, :], preferred_element_type=F32)
        acc_dt = acc_dt + lax.dot_general(
            scaled, dtw_ref[:, span_k], NT, preferred_element_type=F32
        )
    r_in = lax.rsqrt(squares / d_model + 1e-06)

    def slabs_of(value):
        return [value[j * seqs : (j + 1) * seqs] for j in range(props)]

    def rounded(value):
        return value.astype(BF16).astype(F32)

    b_conv = conv(
        slabs_of(rounded(acc_b * r_in)),
        previous(lambda w: bsave_ref[w].astype(F32)),
        lambda k: btap_ref[k],
    )
    c_conv = conv(
        slabs_of(rounded(acc_c * r_in)),
        previous(lambda w: csave_ref[w].astype(F32)),
        lambda k: ctap_ref[k],
    )
    for j in range(props):
        cs[pl.ds(j, seqs, stride=props), :] = c_conv[j]

    raw = acc_dt * r_in + offset_ref[...]
    step_size = slabs_of(jnp.maximum(raw, 0.0) + jnp.log1p(jnp.exp(-jnp.abs(raw))))
    rate = jnp.exp(shrink_ref[...])
    fade = [turn(fade_ref[j]) - rate * step_size[j] for j in range(props)]
    level = [
        sum(lineage[j, i] * fade[i] for i in range(j + 1)) for j in range(props)
    ]
    pairs = [(j, i) for j in range(props) for i in range(j + 1)]
    table = []
    for j, i in pairs:
        score = jnp.sum(c_conv[j] * b_conv[i], axis=1, keepdims=True)
        table.append(
            lineage[j, i] * jnp.exp(jnp.minimum(level[j] - level[i], 0.0)) * score * step_size[i]
            + (bypass_ref[...] if i == j else 0.0)
        )
    table += [jnp.exp(level[j]) for j in range(props)]
    table = jnp.concatenate(table, axis=0)
    table_hi = table.astype(BF16)
    table_lo = (table - table_hi.astype(F32)).astype(BF16)

    for copy in st_loads:
        copy.wait()
    pack = 8 // props
    order2 = order
    second = {}
    second_sib = {}
    lanes = 128
    for ch in range(chunks):
        cols = slice(ch * cw, (ch + 1) * cw)

        def group(g, carry):
            at = pl.multiple_of(g * 8, 8)
            reads = cs[pl.ds(at, 8), :].astype(BF16)
            row = lax.broadcasted_iota(jnp.int32, (8, cw), 0)
            total = None
            for k in range(pack):
                state = st[g * pack + k, ch * cw : (ch + 1) * cw, :].astype(BF16)
                part = lax.dot_general(reads, state, NT, preferred_element_type=F32)
                total = part if total is None else jnp.where(row < k * props, total, part)
            for lane in range(cw // lanes):
                ys[lane, pl.ds(at, 8), :] = total[:, lane * lanes : (lane + 1) * lanes]
            return carry

        def block(q, carry):
            for k in range(4):
                group(q * 4 + k, 0)
            return carry

        lax.fori_loop(0, seqs // pack // 4, block, 0)

        spread = (
            lax.broadcasted_iota(jnp.int32, (heads, cw), 0)
            == (lax.broadcasted_iota(jnp.int32, (heads, cw), 1) + ch * cw) // hd
        ).astype(BF16)
        mix = jnp.dot(table_hi, spread, preferred_element_type=F32) + jnp.dot(
            table_lo, spread, preferred_element_type=F32
        )
        x_conv = conv(
            slabs_of(rounded(acc_x[:, cols] * r_in)),
            previous(lambda w: xsave_ref[w, :, cols].astype(F32)),
            lambda k: xtap_ref[k : k + 1, cols],
        )
        gate = slabs_of(silu(rounded(acc_z[:, cols] * r_in)))
        for j in range(props):
            carried = jnp.concatenate(
                [ys[lane, pl.ds(j, seqs, stride=props), :] for lane in range(cw // lanes)], axis=1
            )
            at = (len(pairs) + j) * seqs
            y = mix[at : at + seqs] * carried
            for index, (to, i) in enumerate(pairs):
                if to == j:
                    y = y + mix[index * seqs : (index + 1) * seqs] * x_conv[i]
            gg[0, tp, ch, pl.ds(j * seqs, seqs), :] = (y * gate[j]).astype(BF16)
        for step in order2:
            second[step, ch] = to_chip(
                gg.at[0, tp, ch], gg.at[n - step, tp, ch], step,
                s2.at[step, ch], r2.at[n - step, ch],
            )
            second[step, ch].start()
        second_sib[0, ch] = to_sibling(gg.at[0, tp, ch], s2b.at[0, ch], r2b.at[0, ch])
        second_sib[0, ch].start()

    loads[4].wait()
    product = jnp.zeros((rows, fl.shape[3]), F32)
    total_sq = jnp.zeros((rows, 1), F32)

    def add_piece(product, total_sq, slot, core, ch):
        value = gg[slot, core, ch]
        chip = lax.rem(kv + slot, n)
        weight = fl[pl.ds(chip * heads + ch * hpc, hpc), core].reshape(cw, fl.shape[3])
        product = product + jnp.dot(value, weight, preferred_element_type=F32)
        value = value.astype(F32)
        return product, total_sq + jnp.sum(value * value, axis=1, keepdims=True)

    for ch in range(chunks):
        product, total_sq = add_piece(product, total_sq, 0, tp, ch)
    for ch in range(chunks):
        to_sibling(gg.at[0, other, ch], s2b.at[0, ch], r2b.at[0, ch]).wait_recv()
        product, total_sq = add_piece(product, total_sq, 0, other, ch)
    arrivals = [(n - step, ch) for step in order for ch in range(chunks)]
    for slot, ch in arrivals:
        to_chip(
            gg.at[0, tp, ch], gg.at[slot, tp, ch], 1, s2.at[0, ch], r2.at[slot, ch]
        ).wait_recv()
        second_sib[slot, ch] = to_sibling(gg.at[slot, tp, ch], s2b.at[slot, ch], r2b.at[slot, ch])
        second_sib[slot, ch].start()
        product, total_sq = add_piece(product, total_sq, slot, tp, ch)
        to_sibling(gg.at[slot, other, ch], s2b.at[slot, ch], r2b.at[slot, ch]).wait_recv()
        product, total_sq = add_piece(product, total_sq, slot, other, ch)
    r_out = lax.rsqrt(total_sq / (heads_all * hd) + 1e-05)
    out_ref[...] = (product * r_out).astype(BF16)
    for copy in list(first.values()) + list(first_sib.values()):
        copy.wait_send()
    for copy in list(second.values()) + list(second_sib.values()):
        copy.wait_send()


def shards(
    candidate_vectors,
    leading_scaling_factor,
    lane_feed_matrix,
    final_valve_matrix,
    increment_matrix,
    entry_basis_matrix,
    readout_basis_matrix,
    lane_feed_kernel,
    entry_basis_kernel,
    readout_basis_kernel,
    increment_offset,
    shrink_speed_exponent,
    lane_bypass_factor,
    final_linear_matrix,
    hidden_carried_memory,
    lane_filter_memory,
    entry_basis_memory,
    readout_basis_memory,
    predecessor_index,
    admitted_counts,
    surplus_fading,
):
    seqs, props, feat = candidate_vectors.shape
    heads = increment_offset.shape[0]
    hd = lane_feed_matrix.shape[3]
    d_model = lane_feed_matrix.shape[0]
    state = hidden_carried_memory.shape[4]
    window = lane_filter_memory.shape[1]
    heads_all, groups, _, out_cols = final_linear_matrix.shape
    n = lax.axis_size("kv")
    rows = seqs * props
    wide = heads * hd
    chunks = max(1, wide // 256)
    cw = wide // chunks
    x = candidate_vectors.transpose(1, 0, 2).reshape(rows, feat)
    wx = lane_feed_matrix.transpose(1, 2, 3, 0).reshape(wide, d_model)
    wz = final_valve_matrix.transpose(1, 2, 3, 0).reshape(wide, d_model)
    dtw = lax.dynamic_slice(
        increment_matrix.transpose(1, 2, 0),
        (lax.axis_index("kv") * heads, lax.axis_index("tp"), 0),
        (heads, 1, d_model),
    ).reshape(heads, d_model)
    wb = entry_basis_matrix.reshape(d_model, state)
    wc = readout_basis_matrix.reshape(d_model, state)
    xsave = (
        lane_filter_memory.reshape(seqs, window, heads, hd)
        .transpose(1, 0, 2, 3)
        .reshape(window, seqs, wide)
    )
    args = (
        x,
        leading_scaling_factor.reshape(1, d_model),
        wx,
        wz,
        dtw,
        wb,
        wc,
        lane_feed_kernel.reshape(CONV, wide),
        entry_basis_kernel,
        readout_basis_kernel,
        increment_offset.reshape(1, heads),
        shrink_speed_exponent.reshape(1, heads),
        lane_bypass_factor.reshape(1, heads),
        final_linear_matrix,
        hidden_carried_memory.reshape(seqs, wide, state),
        xsave,
        entry_basis_memory.transpose(1, 2, 0, 3).reshape(window, seqs, state),
        readout_basis_memory.transpose(1, 2, 0, 3).reshape(window, seqs, state),
        predecessor_index.T,
        admitted_counts.reshape(1, seqs),
        surplus_fading.transpose(1, 2, 3, 0).reshape(props, heads, seqs),
    )
    in_hbm = {0, 2, 3, 5, 6, 13, 14}
    vmem = pl.BlockSpec(memory_space=pltpu.VMEM)
    anywhere = pl.BlockSpec(memory_space=pl.ANY)
    dma = pltpu.SemaphoreType.DMA
    mixed = pl.pallas_call(
        functools.partial(
            mixer_kernel, n, seqs, props, heads, hd, chunks, d_model, heads_all * groups
        ),
        out_shape=jax.ShapeDtypeStruct((rows, out_cols), BF16),
        in_specs=[anywhere if k in in_hbm else vmem for k in range(len(args))],
        out_specs=vmem,
        scratch_shapes=[
            pltpu.VMEM((n, 2, rows, feat), BF16),
            pltpu.VMEM((n, 2, chunks, rows, cw), BF16),
            pltpu.VMEM((wide, d_model), BF16),
            pltpu.VMEM((wide, d_model), BF16),
            pltpu.VMEM((d_model, state), BF16),
            pltpu.VMEM((d_model, state), BF16),
            pltpu.VMEM(final_linear_matrix.shape, BF16),
            pltpu.VMEM((seqs, wide, state), F32),
            pltpu.VMEM((rows, wide), F32),
            pltpu.VMEM((rows, wide), F32),
            pltpu.VMEM((8, 128), F32),
            pltpu.VMEM((rows, state), F32),
            pltpu.VMEM((cw // 128, rows, 128), F32),
            dma((5,)),
            dma((4,)),
            dma,
            dma((n,)),
            dma((n,)),
            dma((n,)),
            dma((n,)),
            dma((n, chunks)),
            dma((n, chunks)),
            dma((n, chunks)),
            dma((n, chunks)),
        ],
        compiler_params=pltpu.CompilerParams(collective_id=0, has_side_effects=True),
    )(*args)
    return mixed.reshape(props, seqs, out_cols).transpose(1, 0, 2)


def solution(mesh):
    placed = (
        P(("grp", "dp"), None, ("kv", "tp")),
        P(),
        P(None, "kv", "tp", None),
        P(None, "kv", "tp", None),
        P(),
        P(None, "tp", None),
        P(None, "tp", None),
        P(None, "kv", "tp", None),
        P(None, "tp", None),
        P(None, "tp", None),
        P("kv", "tp"),
        P("kv", "tp"),
        P("kv", "tp"),
        P(None, None, None, ("kv", "tp")),
        P(("grp", "dp"), "kv", "tp", None, None),
        P(("grp", "dp"), None, "kv", "tp", None),
        P(("grp", "dp"), None, "tp", None),
        P(("grp", "dp"), None, "tp", None),
        P(("grp", "dp"), None),
        P(("grp", "dp")),
        P(("grp", "dp"), None, "kv", "tp"),
    )
    return jax.shard_map(
        shards,
        mesh=mesh,
        in_specs=placed,
        out_specs=P(("grp", "dp"), None, ("kv", "tp")),
        check_vma=False,
    )
```

time: 126 us -> 44.1 us (0.35); the launches traced: 124 us -> 43.7 us
  matrix products: 52.5 us -> 0 us
  Pallas kernels: 0 us -> 33.2 us
  blocking collectives: 24.3 us -> 0 us
  between operations: 14 us -> 0.03 us
  local copies, waits for them, and re-layouts: 21.2 us -> 9.22 us
  waiting for transfers between devices: 8.33 us -> 0 us
  other arithmetic: 3.44 us -> 1.32 us
    dot_general x34 -> x0, matrix products: 52.5 us -> none  [the longest x1 22.1 us: shards(): jnp.einsum('shgpn,sjgn->sjhgp', hidden_carried_memory, c_conv, precision=...]
    pallas_call x0 -> x1, Pallas kernels: none -> 33.2 us  [shards(): pl.pallas_call(functools.partial(mixer_kernel, n, seqs, props, heads, hd,...]
    all_gather x1 -> x0, blocking collectives: 12.7 us -> none  [shards(): piece = lax.all_gather(candidate_vectors, ('kv', 'tp'), axis=2, tiled=True)]
    psum x1 -> x0, blocking collectives: 11.6 us -> none  [shards(): sumsq_start = lax.psum(jnp.sum(gated_f * gated_f, axis=1), ('kv', 'tp'))]
    all_gather x1 -> x0, waiting for transfers between devices: 8.31 us -> none  [shards(): lax.all_gather(gated, ('kv', 'tp'), axis=1, tiled=True)]
    gather x15 -> x0, local copies, waits for them, and re-layouts: 5.63 us -> none  [lineage_tables(): jnp.take_along_axis(predecessor_index, jnp.maximum(current, 0), axis=1)]
    mul x8 -> x0, local copies, waits for them, and re-layouts: 2.5 us -> none  [the longest x6 1.48 us: conv_tree(): total = total + taps[CONV - 1 - lag] * value]
    reshape x6 -> x5, local copies, waits for them, and re-layouts: 3.23 us -> 5.58 us  [the longest x2 2.1 us: shards(): xsave = lane_filter_memory.reshape(seqs, window, heads, hd).transpose(1,...]
  transfers between devices with their start and end apart: 1 -> 0, of which waited for: 1 -> 0; matrix products, arithmetic and copies ran while one was open for 3% -> 0% of each run, Pallas kernels for 0% -> 0%
where the time goes in v1:
time: 44.1 us; the launch traced here: 43.7 us
  Pallas kernels  33.2 us (75%)
  local copies, waits for them, and re-layouts  9.22 us (21%)
  other arithmetic  1.32 us (3%)
    pallas_call x1, Pallas kernels, shards(): pl.pallas_call(functools.partial(mixer_kernel, n, seqs, props, heads, hd,...  33.2 us
    reshape x2, local copies, waits for them, and re-layouts, shards(): xsave = lane_filter_memory.reshape(seqs, window, heads, hd).transpose(1,...  2.1 us
    unnamed x4, local copies, waits for them, and re-layouts  2.09 us
    reshape x1, local copies, waits for them, and re-layouts, shards(): return mixed.reshape(props, seqs, out_cols).transpose(1, 0, 2)  1.52 us
    transpose x1, local copies, waits for them, and re-layouts, shards(): x = candidate_vectors.transpose(1, 0, 2).reshape(rows, feat)  1.48 us
    unnamed x1, other arithmetic  1.32 us
    reshape x1, local copies, waits for them, and re-layouts, shards(): leading_scaling_factor.reshape(1, d_model)  1.28 us

profile of v1, /device:TPU:19, one launch (start us, length us, event | category | flops | bytes accessed | tf_op | source)
XLA Modules:
  0.0 43.7 jit_solution(14683436265164623892)
XLA Ops:
  0.0 0.0 copy-start
  0.0 0.9 %copy-done = bf16[2048,32,2]{0,2,1:T(2,128)(2,1)S(1)} copy-done((bf16[2048,32,2]{0,2,1:T(2,128)(2,1)S(1)}, bf16[2048,32,2]{0,2,1:T(2,128)(2,1)}, u32[]{:S(2)}) %copy-start) | copy-done | bytes 262168
  1.0 0.1 constant_dynamic-slice_fusion
  1.0 0.6 %copy.34 = bf16[2048,8,1]{0,1,2:T(8,128)(2,1)} copy(bf16[2048,8,1]{0,2,1:T(2,128)(2,1)S(1)} %constant_dynamic-slice_fusion) | data formatting | bytes 65536
  1.7 1.3 %reshape.76 = bf16[7,32,512]{2,0,1:T(8,128)(2,1)S(1)} reshape(bf16[7,32,8,64]{3,2,0,1:T(8,128)(2,1)} %bitcast.52) | data formatting | bytes 458752 | tf_op jit(solution)/shard_map/reshape | solution.py:363
  3.0 0.8 %copy.29.xsave_ref = bf16[7,32,512]{2,1,0:T(8,128)(2,1)} copy(bf16[7,32,512]{2,0,1:T(8,128)(2,1)S(1)} %reshape.76) | data formatting | bytes 458752 | tf_op jit(solution)/shard_map/reshape | solution.py:363
  3.8 1.5 %copy.22 = bf16[4,32,256]{2,1,0:T(8,128)(2,1)} copy(bf16[4,32,256]{2,0,1:T(4,128)(2,1)} %bitcast.56) | data formatting | bytes 131072 | tf_op jit(solution)/shard_map/transpose | solution.py:350
  5.2 0.5 %broadcast.3 = f32[]{:T(128)} broadcast(f32[]{:T(128)} %constant.34), dimensions={} | broadcast | bytes 8 | tf_op args[7]
  5.8 1.3 %reduce.3 = f32[4,8,64]{2,1,0:T(8,128)S(1)} reduce(f32[4,8,1,64]{3,2,1,0:T(1,128)} %param.28, f32[]{:T(128)} %broadcast.3), dimensions={2}, to_apply=%param.28.reduce_sub_computation.3 | reduce | bytes 16388 | tf_op args[7]
  7.1 0.7 %reshape.64.xtap_ref = f32[4,512]{1,0:T(4,128)} reshape(f32[4,8,64]{2,1,0:T(8,128)S(1)} %reduce.3) | data formatting | bytes 16384 | tf_op jit(solution)/shard_map/reshape | solution.py:373
  7.8 1.3 %reshape.58.gain_ref = bf16[1,2048]{1,0:T(2,128)(2,1)} reshape(bf16[2048]{0:T(1024)(128)(2,1)} %param.22) | data formatting | bytes 8192 | tf_op jit(solution)/shard_map/reshape | solution.py:367
  9.0 33.2 %shard_map.199 = bf16[128,256]{1,0:T(8,128)(2,1)} custom-call(bf16[128,256]{1,0:T(8,128)(2,1)} %bitcast.53, bf16[1,2048]{1,0:T(2,128)(2,1)} %reshape.58.gain_ref, bf16[512,2048]{1,0:T(8,128)(2,1)} %bitcast.48, bf16[512,2048]{1,0:T(8,128)(2,1)} %bitcast.49, bf16[8,2048]{1,0:T(8,128)(2,1)} %bitcast.55, bf16[2048,128]{1,0:T(8,128)(2,1)} %bitcast.50, ...), custom_call_target="tpu_custom_call" | custom-call | tf_op jit(solution)/shard_map/pallas_call | solution.py:392
  42.2 1.5 %copy.33 = bf16[4,32,256]{2,0,1:T(4,128)(2,1)} copy(bf16[4,32,256]{2,1,0:T(8,128)(2,1)} %bitcast.54) | data formatting | bytes 131072 | tf_op jit(solution)/shard_map/reshape | solution.py:427
Async XLA Ops:
  0.0 1.0 %copy-start = (bf16[2048,32,2]{0,2,1:T(2,128)(2,1)S(1)}, bf16[2048,32,2]{0,2,1:T(2,128)(2,1)}, u32[]{:S(2)}) copy-start(bf16[2048,32,2]{0,2,1:T(2,128)(2,1)} %param.25) | copy-start | bytes 786436

commit v2 on v1

--- a/solution.py
+++ b/solution.py
@@ -21,23 +21,25 @@
 
 def mixer_kernel(
     n, seqs, props, heads, hd, chunks, d_model, heads_all,
-    x_hbm, gain_ref, wx_hbm, wz_hbm, dtw_ref, wb_hbm, wc_hbm,
+    x_hbm, gain_ref, wx_hbm, wz_hbm, inc_hbm, wb_hbm, wc_hbm,
     xtap_ref, btap_ref, ctap_ref, offset_ref, shrink_ref, bypass_ref,
-    fl_hbm, st_hbm, xsave_ref, bsave_ref, csave_ref, pred_ref, adm_ref, fade_ref,
+    fl_hbm, st_hbm, xsave_hbm, bsave_ref, csave_ref, pred_ref, adm_ref, slot_ref, fade_ref,
     out_ref,
-    xg, gg, wx, wz, wb, wc, fl, st, acc_x, acc_z, xrow, cs, ys,
+    xg, gg, wx, wz, wb, wc, fl, st, acc_x, acc_z, cs, ys,
+    xin, xrow, gain, inc, inc_rows, dtw, xsave, xprev,
     load_sem, st_sem, own_sem, s1, r1, s1b, r1b, s2, r2, s2b, r2b,
 ):
     kv = lax.axis_index("kv")
     tp = lax.axis_index("tp")
     other = 1 - tp
     rows = seqs * props
-    feat = x_hbm.shape[1]
+    feat = x_hbm.shape[2]
+    lanes = 128
     wide = heads * hd
     cw = wide // chunks
     hpc = heads // chunks
 
-    own = pltpu.make_async_copy(x_hbm, xg.at[0, tp], own_sem)
+    own = pltpu.make_async_copy(x_hbm, xin, own_sem)
     own.start()
     barrier = pltpu.get_barrier_semaphore()
     for step in range(1, n):
@@ -48,7 +50,15 @@
 
     loads = []
     for index, (src, dst) in enumerate(
-        ((wb_hbm, wb), (wc_hbm, wc), (wx_hbm, wx), (wz_hbm, wz), (fl_hbm, fl))
+        (
+            (wb_hbm, wb),
+            (wc_hbm, wc),
+            (wx_hbm, wx),
+            (wz_hbm, wz),
+            (inc_hbm.at[pl.ds(kv * heads, heads)], inc),
+            (xsave_hbm, xsave),
+            (fl_hbm, fl),
+        )
     ):
         loads.append(pltpu.make_async_copy(src, dst, load_sem.at[index]))
     parts = st_sem.shape[0]
@@ -59,11 +69,23 @@
         )
         for part in range(parts)
     ]
-    for copy in loads[:4] + st_loads + loads[4:]:
+    for copy in loads[:6] + st_loads + loads[6:]:
         copy.start()
 
+    own.wait()
+    tiles = xrow.shape[0]
+    tile_w = feat // tiles
+    for s in range(seqs):
+        for tile in range(tiles):
+            xrow[tile, s * props : (s + 1) * props, :tile_w] = xin[
+                s, :, tile * tile_w : (tile + 1) * tile_w
+            ].astype(F32)
+    for j in range(props):
+        for tile in range(tiles):
+            xg[0, tp, j * seqs : (j + 1) * seqs, tile * tile_w : (tile + 1) * tile_w] = xrow[
+                tile, pl.ds(j, seqs, stride=props), :
+            ][:, :tile_w].astype(BF16)
     pl.semaphore_wait(barrier, n)
-    own.wait()
 
     def to_chip(src, dst, step, send, recv):
         return pltpu.make_async_remote_copy(
@@ -118,7 +140,7 @@
     depth_is = {
         (j, d): (depth[j] == float(d)).astype(F32) for j in range(props) for d in range(j + 1)
     }
-    slots = xsave_ref.shape[0]
+    slots = bsave_ref.shape[0]
     pick = [(admitted == float(a)).astype(F32) for a in range(slots - CONV + 2)]
 
     def previous(save):
@@ -143,12 +165,26 @@
             result.append(silu(total))
         return result
 
-    for copy in loads[:4]:
+    for copy in loads[:6]:
         copy.wait()
+    gain[...] = gain_ref[...].astype(F32)
+    for h in range(heads):
+        inc_rows[2 * h : 2 * h + 2, :] = inc[h].astype(F32)
+    dtw[...] = inc_rows[...].astype(BF16)
+
+    def pick_rows(block, carry):
+        for k in range(4):
+            s = block * 4 + k
+            for back in range(CONV - 1):
+                at = pl.multiple_of(s * heads, heads)
+                xprev[back, pl.ds(at, heads), :hd] = xsave[s, slot_ref[s] + back].astype(F32)
+        return carry
+
+    lax.fori_loop(0, seqs // 4, pick_rows, 0)
     squares = jnp.zeros((rows, 1), F32)
     acc_b = jnp.zeros((rows, wb.shape[1]), F32)
     acc_c = jnp.zeros((rows, wc.shape[1]), F32)
-    acc_dt = jnp.zeros((rows, heads), F32)
+    acc_dt = jnp.zeros((rows, 2 * heads), F32)
     for place, slot in enumerate([0] + [n - step for step in order]):
         if slot:
             to_chip(xg.at[0, tp], xg.at[slot, tp], 1, s1.at[0], r1.at[slot]).wait_recv()
@@ -160,7 +196,11 @@
         tokens = jnp.concatenate([xg[slot, 0], xg[slot, 1]], axis=1).astype(F32)
         squares = squares + jnp.sum(tokens * tokens, axis=1, keepdims=True)
         span_k = pl.ds(base, 2 * feat)
-        scaled = (tokens * gain_ref[:, span_k].astype(F32)).astype(BF16)
+        gain_rows = 2 * feat // lanes
+        gains = jnp.concatenate(
+            [gain[pl.ds(chip * gain_rows + k, 1), :] for k in range(gain_rows)], axis=1
+        )
+        scaled = (tokens * gains).astype(BF16)
         px = lax.dot_general(scaled, wx[:, span_k], NT, preferred_element_type=F32)
         pz = lax.dot_general(scaled, wz[:, span_k], NT, preferred_element_type=F32)
         if place == 0:
@@ -172,7 +212,7 @@
         acc_b = acc_b + jnp.dot(scaled, wb[span_k, :], preferred_element_type=F32)
         acc_c = acc_c + jnp.dot(scaled, wc[span_k, :], preferred_element_type=F32)
         acc_dt = acc_dt + lax.dot_general(
-            scaled, dtw_ref[:, span_k], NT, preferred_element_type=F32
+            scaled, dtw[:, span_k], NT, preferred_element_type=F32
         )
     r_in = lax.rsqrt(squares / d_model + 1e-06)
 
@@ -195,6 +235,11 @@
     for j in range(props):
         cs[pl.ds(j, seqs, stride=props), :] = c_conv[j]
 
+    mine = (
+        lax.broadcasted_iota(jnp.int32, (2 * heads, heads), 0)
+        == 2 * lax.broadcasted_iota(jnp.int32, (2 * heads, heads), 1) + tp
+    ).astype(F32)
+    acc_dt = jnp.dot(acc_dt, mine, precision=HIGH, preferred_element_type=F32)
     raw = acc_dt * r_in + offset_ref[...]
     step_size = slabs_of(jnp.maximum(raw, 0.0) + jnp.log1p(jnp.exp(-jnp.abs(raw))))
     rate = jnp.exp(shrink_ref[...])
@@ -221,7 +266,6 @@
     order2 = order
     second = {}
     second_sib = {}
-    lanes = 128
     for ch in range(chunks):
         cols = slice(ch * cw, (ch + 1) * cw)
 
@@ -254,8 +298,19 @@
         )
         x_conv = conv(
             slabs_of(rounded(acc_x[:, cols] * r_in)),
-            previous(lambda w: xsave_ref[w, :, cols].astype(F32)),
-            lambda k: xtap_ref[k : k + 1, cols],
+            [
+                jnp.concatenate(
+                    [
+                        xprev[back, pl.ds(ch * hpc + h, seqs, stride=heads), :][:, :hd]
+                        for h in range(hpc)
+                    ],
+                    axis=1,
+                )
+                for back in range(CONV - 1)
+            ],
+            lambda k: jnp.concatenate(
+                [xtap_ref[k, ch * hpc + h] for h in range(hpc)], axis=1
+            ),
         )
         gate = slabs_of(silu(rounded(acc_z[:, cols] * r_in)))
         for j in range(props):
@@ -277,7 +332,7 @@
         second_sib[0, ch] = to_sibling(gg.at[0, tp, ch], s2b.at[0, ch], r2b.at[0, ch])
         second_sib[0, ch].start()
 
-    loads[4].wait()
+    loads[6].wait()
     product = jnp.zeros((rows, fl.shape[3]), F32)
     total_sq = jnp.zeros((rows, 1), F32)
 
@@ -347,30 +402,19 @@
     wide = heads * hd
     chunks = max(1, wide // 256)
     cw = wide // chunks
-    x = candidate_vectors.transpose(1, 0, 2).reshape(rows, feat)
     wx = lane_feed_matrix.transpose(1, 2, 3, 0).reshape(wide, d_model)
     wz = final_valve_matrix.transpose(1, 2, 3, 0).reshape(wide, d_model)
-    dtw = lax.dynamic_slice(
-        increment_matrix.transpose(1, 2, 0),
-        (lax.axis_index("kv") * heads, lax.axis_index("tp"), 0),
-        (heads, 1, d_model),
-    ).reshape(heads, d_model)
     wb = entry_basis_matrix.reshape(d_model, state)
     wc = readout_basis_matrix.reshape(d_model, state)
-    xsave = (
-        lane_filter_memory.reshape(seqs, window, heads, hd)
-        .transpose(1, 0, 2, 3)
-        .reshape(window, seqs, wide)
-    )
     args = (
-        x,
-        leading_scaling_factor.reshape(1, d_model),
+        candidate_vectors,
+        leading_scaling_factor.reshape(d_model // 128, 128),
         wx,
         wz,
-        dtw,
+        increment_matrix.transpose(1, 2, 0),
         wb,
         wc,
-        lane_feed_kernel.reshape(CONV, wide),
+        lane_feed_kernel,
         entry_basis_kernel,
         readout_basis_kernel,
         increment_offset.reshape(1, heads),
@@ -378,23 +422,30 @@
         lane_bypass_factor.reshape(1, heads),
         final_linear_matrix,
         hidden_carried_memory.reshape(seqs, wide, state),
-        xsave,
+        lane_filter_memory.reshape(seqs, window, heads, hd),
         entry_basis_memory.transpose(1, 2, 0, 3).reshape(window, seqs, state),
         readout_basis_memory.transpose(1, 2, 0, 3).reshape(window, seqs, state),
         predecessor_index.T,
         admitted_counts.reshape(1, seqs),
+        admitted_counts,
         surplus_fading.transpose(1, 2, 3, 0).reshape(props, heads, seqs),
     )
-    in_hbm = {0, 2, 3, 5, 6, 13, 14}
+    in_hbm = {0, 2, 3, 4, 5, 6, 13, 14, 15}
+    in_smem = 20
     vmem = pl.BlockSpec(memory_space=pltpu.VMEM)
     anywhere = pl.BlockSpec(memory_space=pl.ANY)
+    scalars = pl.BlockSpec(memory_space=pltpu.SMEM)
     dma = pltpu.SemaphoreType.DMA
+    tiles = max(1, feat // 128)
     mixed = pl.pallas_call(
         functools.partial(
             mixer_kernel, n, seqs, props, heads, hd, chunks, d_model, heads_all * groups
         ),
         out_shape=jax.ShapeDtypeStruct((rows, out_cols), BF16),
-        in_specs=[anywhere if k in in_hbm else vmem for k in range(len(args))],
+        in_specs=[
+            anywhere if k in in_hbm else scalars if k == in_smem else vmem
+            for k in range(len(args))
+        ],
         out_specs=vmem,
         scratch_shapes=[
             pltpu.VMEM((n, 2, rows, feat), BF16),
@@ -407,10 +458,17 @@
             pltpu.VMEM((seqs, wide, state), F32),
             pltpu.VMEM((rows, wide), F32),
             pltpu.VMEM((rows, wide), F32),
-            pltpu.VMEM((8, 128), F32),
             pltpu.VMEM((rows, state), F32),
             pltpu.VMEM((cw // 128, rows, 128), F32),
-            dma((5,)),
+            pltpu.VMEM((seqs, props, feat), BF16),
+            pltpu.VMEM((tiles, rows, 128), F32),
+            pltpu.VMEM((d_model // 128, 128), F32),
+            pltpu.VMEM((heads, groups, d_model), BF16),
+            pltpu.VMEM((heads * groups, d_model), F32),
+            pltpu.VMEM((heads * groups, d_model), BF16),
+            pltpu.VMEM((seqs, window, heads, hd), BF16),
+            pltpu.VMEM((CONV - 1, seqs * heads, 128), F32),
+            dma((7,)),
             dma((4,)),
             dma,
             dma((n,)),

time: 44.1 us -> 35.1 us (0.80)
  local copies, waits for them, and re-layouts: 9.22 us -> 1.52 us
  other arithmetic: 1.32 us -> 0 us
    reshape x4 -> x0, local copies, waits for them, and re-layouts: 4.05 us -> none  [the longest x2 2.1 us: shards(): xsave = lane_filter_memory.reshape(seqs, window, heads, hd).transpose(1,...]
    unnamed x4 -> x0, local copies, waits for them, and re-layouts: 2.09 us -> none
    transpose x1 -> x0, local copies, waits for them, and re-layouts: 1.48 us -> none  [shards(): x = candidate_vectors.transpose(1, 0, 2).reshape(rows, feat)]
    unnamed x1 -> x0, other arithmetic: 1.32 us -> none
where the time goes in v2:
time: 35.1 us; the launch traced here: 34.9 us
  Pallas kernels  33.3 us (95%)
  local copies, waits for them, and re-layouts  1.52 us (4%)
    pallas_call x1, Pallas kernels, shards(): pl.pallas_call(functools.partial(mixer_kernel, n, seqs, props, heads, hd,...  33.3 us
    reshape x1, local copies, waits for them, and re-layouts, shards(): return mixed.reshape(props, seqs, out_cols).transpose(1, 0, 2)  1.52 us

profile of v2, /device:TPU:19, one launch (start us, length us, event | category | flops | bytes accessed | tf_op | source)
XLA Modules:
  0.0 34.9 jit_solution(2607374259534808635)
XLA Ops:
  0.0 33.3 %shard_map.199 = bf16[128,256]{1,0:T(8,128)(2,1)} custom-call(bf16[32,4,256]{2,1,0:T(4,128)(2,1)} %x_hbm.1, bf16[16,128]{1,0:T(8,128)(2,1)} %bitcast.47, bf16[512,2048]{1,0:T(8,128)(2,1)} %bitcast.37, bf16[512,2048]{1,0:T(8,128)(2,1)} %bitcast.38, bf16[32,2,2048]{2,1,0:T(2,128)(2,1)} %bitcast.42, bf16[2048,128]{1,0:T(8,128)(2,1)} %bitcast.39, ...), custom_call_target="tpu_custom_call" | custom-call | tf_op jit(solution)/shard_map/pallas_call | solution.py:440
  33.3 1.5 %copy.27 = bf16[4,32,256]{2,0,1:T(4,128)(2,1)} copy(bf16[4,32,256]{2,1,0:T(8,128)(2,1)} %bitcast.43) | data formatting | bytes 131072 | tf_op jit(solution)/shard_map/reshape | solution.py:485

commit v3 on v2

--- a/solution.py
+++ b/solution.py
@@ -27,7 +27,7 @@
     out_ref,
     xg, gg, wx, wz, wb, wc, fl, st, acc_x, acc_z, cs, ys,
     xin, xrow, gain, inc, inc_rows, dtw, xsave, xprev,
-    load_sem, st_sem, own_sem, s1, r1, s1b, r1b, s2, r2, s2b, r2b,
+    load_sem, st_sem, own_sem, s1, r1, s1b, r1b, s2, r2, s2b, r2b, p1, p2,
 ):
     kv = lax.axis_index("kv")
     tp = lax.axis_index("tp")
@@ -99,13 +99,45 @@
             device_id={"tp": other}, device_id_type=MESH,
         )
 
-    order = sorted(range(1, n), key=lambda step: (min(step, n - step), step))
+    relayed = n > 3
+
+    def direct(step, action):
+        if relayed and step == n - 1:
+            pl.when(kv != 0)(action)
+        elif relayed and step == 1:
+            pl.when(kv != n - 1)(action)
+        else:
+            action()
+
+    def passed(slot, view, send, recv):
+        if not relayed:
+            return []
+        result = []
+        if isinstance(slot, int) and slot == 2:
+            result.append((kv == n - 2, to_chip(view(2), view(1), 1, send, recv(1))))
+        if isinstance(slot, int) and slot == n - 2:
+            result.append((kv == 1, to_chip(view(n - 2), view(n - 1), n - 1, send, recv(n - 1))))
+        return result
+
+    forwards = []
+
+    def pass_on(slot, view, send, recv):
+        for here, copy in passed(slot, view, send, recv):
+            pl.when(here)(copy.start)
+            forwards.append((here, copy))
+
+    middle = sorted({2, n - 2}) + list(range(3, n - 2)) if relayed else []
+    order = middle + [step for step in range(1, n) if step not in middle]
+    arrivals = [n - step for step in order]
+    if relayed:
+        near = jnp.where(kv == n - 1, n - 1, 1)
+        arrivals = middle + [near, n - near]
     first = {}
     for step in order:
         first[step] = to_chip(
             xg.at[0, tp], xg.at[n - step, tp], step, s1.at[step], r1.at[n - step]
         )
-        first[step].start()
+        direct(step, first[step].start)
     first_sib = {0: to_sibling(xg.at[0, tp], s1b.at[0], r1b.at[0])}
     first_sib[0].start()
 
@@ -185,11 +217,12 @@
     acc_b = jnp.zeros((rows, wb.shape[1]), F32)
     acc_c = jnp.zeros((rows, wc.shape[1]), F32)
     acc_dt = jnp.zeros((rows, 2 * heads), F32)
-    for place, slot in enumerate([0] + [n - step for step in order]):
-        if slot:
+    for place, slot in enumerate([0] + arrivals):
+        if place:
             to_chip(xg.at[0, tp], xg.at[slot, tp], 1, s1.at[0], r1.at[slot]).wait_recv()
-            first_sib[slot] = to_sibling(xg.at[slot, tp], s1b.at[slot], r1b.at[slot])
-            first_sib[slot].start()
+            pass_on(slot, lambda k: xg.at[k, tp], p1, lambda k: r1.at[k])
+            first_sib[place] = to_sibling(xg.at[slot, tp], s1b.at[slot], r1b.at[slot])
+            first_sib[place].start()
         to_sibling(xg.at[slot, other], s1b.at[slot], r1b.at[slot]).wait_recv()
         chip = lax.rem(kv + slot, n)
         base = pl.multiple_of(chip * (2 * feat), 2 * feat)
@@ -328,7 +361,7 @@
                 gg.at[0, tp, ch], gg.at[n - step, tp, ch], step,
                 s2.at[step, ch], r2.at[n - step, ch],
             )
-            second[step, ch].start()
+            direct(step, second[step, ch].start)
         second_sib[0, ch] = to_sibling(gg.at[0, tp, ch], s2b.at[0, ch], r2b.at[0, ch])
         second_sib[0, ch].start()
 
@@ -349,22 +382,28 @@
     for ch in range(chunks):
         to_sibling(gg.at[0, other, ch], s2b.at[0, ch], r2b.at[0, ch]).wait_recv()
         product, total_sq = add_piece(product, total_sq, 0, other, ch)
-    arrivals = [(n - step, ch) for step in order for ch in range(chunks)]
-    for slot, ch in arrivals:
+    for place, (slot, ch) in enumerate((slot, ch) for slot in arrivals for ch in range(chunks)):
         to_chip(
             gg.at[0, tp, ch], gg.at[slot, tp, ch], 1, s2.at[0, ch], r2.at[slot, ch]
         ).wait_recv()
-        second_sib[slot, ch] = to_sibling(gg.at[slot, tp, ch], s2b.at[slot, ch], r2b.at[slot, ch])
-        second_sib[slot, ch].start()
+        pass_on(slot, lambda k, ch=ch: gg.at[k, tp, ch], p2.at[ch], lambda k, ch=ch: r2.at[k, ch])
+        second_sib[place + 1, ch] = to_sibling(
+            gg.at[slot, tp, ch], s2b.at[slot, ch], r2b.at[slot, ch]
+        )
+        second_sib[place + 1, ch].start()
         product, total_sq = add_piece(product, total_sq, slot, tp, ch)
         to_sibling(gg.at[slot, other, ch], s2b.at[slot, ch], r2b.at[slot, ch]).wait_recv()
         product, total_sq = add_piece(product, total_sq, slot, other, ch)
     r_out = lax.rsqrt(total_sq / (heads_all * hd) + 1e-05)
     out_ref[...] = (product * r_out).astype(BF16)
-    for copy in list(first.values()) + list(first_sib.values()):
+    for step, copy in first.items():
+        direct(step, copy.wait_send)
+    for (step, _), copy in second.items():
+        direct(step, copy.wait_send)
+    for copy in list(first_sib.values()) + list(second_sib.values()):
         copy.wait_send()
-    for copy in list(second.values()) + list(second_sib.values()):
-        copy.wait_send()
+    for here, copy in forwards:
+        pl.when(here)(copy.wait_send)
 
 
 def shards(
@@ -479,6 +518,8 @@
             dma((n, chunks)),
             dma((n, chunks)),
             dma((n, chunks)),
+            dma,
+            dma((chunks,)),
         ],
         compiler_params=pltpu.CompilerParams(collective_id=0, has_side_effects=True),
     )(*args)

time: 35.1 us -> 34.3 us (0.977)
  the two profiles are of different devices: /device:TPU:19 before, /device:TPU:0 now
where the time goes in v3:
time: 34.3 us; the launch traced here: 34.1 us
  Pallas kernels  32.5 us (95%)
  local copies, waits for them, and re-layouts  1.52 us (4%)
    pallas_call x1, Pallas kernels, shards(): pl.pallas_call(functools.partial(mixer_kernel, n, seqs, props, heads, hd,...  32.5 us
    reshape x1, local copies, waits for them, and re-layouts, shards(): return mixed.reshape(props, seqs, out_cols).transpose(1, 0, 2)  1.52 us

profile of v3, /device:TPU:0, one launch (start us, length us, event | category | flops | bytes accessed | tf_op | source)
XLA Modules:
  0.0 34.1 jit_solution(15282664140925018989)
XLA Ops:
  0.0 32.5 %shard_map.199 = bf16[128,256]{1,0:T(8,128)(2,1)} custom-call(bf16[32,4,256]{2,1,0:T(4,128)(2,1)} %x_hbm.1, bf16[16,128]{1,0:T(8,128)(2,1)} %bitcast.47, bf16[512,2048]{1,0:T(8,128)(2,1)} %bitcast.37, bf16[512,2048]{1,0:T(8,128)(2,1)} %bitcast.38, bf16[32,2,2048]{2,1,0:T(2,128)(2,1)} %bitcast.42, bf16[2048,128]{1,0:T(8,128)(2,1)} %bitcast.39, ...), custom_call_target="tpu_custom_call" | custom-call | tf_op jit(solution)/shard_map/pallas_call | solution.py:479
  32.5 1.5 %copy.27 = bf16[4,32,256]{2,0,1:T(4,128)(2,1)} copy(bf16[4,32,256]{2,1,0:T(8,128)(2,1)} %bitcast.43) | data formatting | bytes 131072 | tf_op jit(solution)/shard_map/reshape | solution.py:526
